TPU v7x, 32 devices: a whole 2x2x4 slice. The times are simulated.
32 devices in a mesh: sp: 4 (over z), dp: 8 (over y, x, core).
Axes of the slice: x: 2, y: 2, z: 4, core: 2. Of those that a mesh axis runs over, the one named last changes fastest.
Arguments:
- queries: bfloat16 [8, 512, 1024], P('dp', 'sp'), may hold values from -300 to 300
- keys: bfloat16 [8, 512, 1024], P('dp', 'sp'), may hold values from -7 to 7
- values: bfloat16 [8, 512, 1024], P('dp', 'sp'), may hold values from -6 to 6
- cum_gates: float32 [8, 16, 512], P('dp', 'sp'), may hold values from -67 to 0, as said below
- out_weight: bfloat16 [1024, 2048], P(None, 'dp'), may hold values from -0.1875 to 0.1875
Outputs:
- mixed: bfloat16 [8, 512, 2048], P('dp', 'sp')
Inputs may be any that keep to these rules, and one draw needn't show every extreme that they name: `cum_gates`: never rises along positions.
All inputs are finite; a program needn't handle non-finite values.
Results may differ from a plain program's by a relative error of at most 0.011.
Values may be sent and summed in bfloat16 or wider, within the bound.
A program may use at most 64 MiB of HBM per device.

v0:
```python
import jax
import jax.numpy as jnp
from jax import lax
from jax.sharding import PartitionSpec as P


def attend_heads(query_loc, key_loc, value_loc, cum_loc):
    length = query_loc.shape[0]
    head_count = cum_loc.shape[0]
    head_size = query_loc.shape[1] // head_count
    query_heads = query_loc.reshape(length, head_count, head_size).transpose(1, 0, 2)
    key_heads = key_loc.reshape(length, head_count, head_size).transpose(1, 0, 2)
    value_heads = value_loc.reshape(length, head_count, head_size).transpose(1, 0, 2)
    block_rows = min(512, length)
    block_count = length // block_rows
    query_blocks = query_heads.reshape(head_count, block_count, block_rows, head_size).transpose(
        1, 0, 2, 3
    )
    cum_blocks = cum_loc.reshape(head_count, block_count, block_rows).transpose(1, 0, 2)
    key_pos = jnp.arange(length)
    score_scale = head_size ** (-0.5)

    def one_block(packed):
        query_block, cum_block, block_index = packed
        scores = (
            jnp.einsum("hqd,hkd->hqk", query_block, key_heads, preferred_element_type=jnp.float32)
            * score_scale
        )
        scores = scores + cum_block[:, :, None] - cum_loc[:, None, :]
        query_pos = block_index * block_rows + jnp.arange(block_rows)
        scores = jnp.where(key_pos[None, :] <= query_pos[:, None], scores, -jnp.inf)
        row_max = jnp.max(scores, axis=-1, keepdims=True)
        expon = jnp.exp(scores - row_max)
        weights = (expon / jnp.sum(expon, axis=-1, keepdims=True)).astype(jnp.bfloat16)
        return jnp.einsum(
            "hqk,hkd->hqd", weights, value_heads, preferred_element_type=jnp.float32
        ).astype(jnp.bfloat16)

    results = lax.map(one_block, (query_blocks, cum_blocks, jnp.arange(block_count)))
    return results.transpose(0, 2, 1, 3).reshape(length, head_count * head_size)


def shards(queries, keys, values, cum_gates, out_weight):
    query_loc, key_loc, value_loc = (
        lax.all_to_all(queries[0], "sp", split_axis=1, concat_axis=0, tiled=True),
        lax.all_to_all(keys[0], "sp", split_axis=1, concat_axis=0, tiled=True),
        lax.all_to_all(values[0], "sp", split_axis=1, concat_axis=0, tiled=True),
    )
    head_out = attend_heads(query_loc, key_loc, value_loc, cum_gates[0])
    token_rows = lax.all_to_all(head_out, "sp", split_axis=0, concat_axis=1, tiled=True)
    mixed_rows = jnp.dot(
        token_rows,
        lax.all_gather(out_weight, "dp", axis=1, tiled=True),
        preferred_element_type=jnp.float32,
    )
    return mixed_rows.astype(jnp.bfloat16)[None]


def solution(mesh):
    in_specs = (
        P("dp", "sp", None),
        P("dp", "sp", None),
        P("dp", "sp", None),
        P("dp", "sp", None),
        P(None, "dp"),
    )
    out_specs = P("dp", "sp", None)
    return jax.shard_map(shards, mesh=mesh, in_specs=in_specs, out_specs=out_specs, check_vma=False)
```

profile of v0, /device:TPU:0, one launch (start us, length us, event | category | flops | bytes accessed | tf_op | source)
XLA Modules:
  0.0 70.6 jit_solution(15589185391512869940)
XLA Ops:
  6.5 0.0 copy-start
  6.5 0.0 all-gather.2.cloned.1.call-start
  6.5 0.7 %all-gather.2.cloned.1.call-update = ((bf16[1024,256]{1,0:T(8,128)(2,1)}), bf16[1024,2048]{1,0:T(8,128)(2,1)}) async-update(((), (), s32[]{:S(2)}) %all-gather.2.cloned.1.call-start, bf16[1024,256]{1,0:T(8,128)(2,1)} %param.9) | async-update | bytes 5242904
  7.3 1.8 %copy.15 = bf16[1,128,1024]{1,2,0:T(8,128)(2,1)} copy(bf16[1,128,1024]{2,1,0:T(8,128)(2,1)} %param.5) | data formatting | bytes 524288 | tf_op args[0]
  9.0 6.3 %all-to-all-start = ((bf16[128,4,256]{0,2,1:T(8,128)(2,1)}), bf16[128,4,256]{0,2,1:T(8,128)(2,1)S(1)}, u32[]{:S(2)}, u32[]{:S(2)}) async-start(bf16[128,4,256]{0,2,1:T(8,128)(2,1)} %bitcast), calls=%async_computation | async-start | bytes 524288 | tf_op jit(solution)/shard_map/all_to_all | solution.py:45
  15.4 1.8 %copy.17 = bf16[1,128,1024]{1,2,0:T(8,128)(2,1)} copy(bf16[1,128,1024]{2,1,0:T(8,128)(2,1)} %param.6) | data formatting | bytes 524288 | tf_op args[1]
  17.2 7.1 %all-to-all-done = bf16[128,4,256]{0,2,1:T(8,128)(2,1)S(1)} async-done(((bf16[128,4,256]{0,2,1:T(8,128)(2,1)}), bf16[128,4,256]{0,2,1:T(8,128)(2,1)S(1)}, u32[]{:S(2)}, u32[]{:S(2)}) %all-to-all-start) | async-done | bytes 262176 | tf_op jit(solution)/shard_map/all_to_all | solution.py:45
  24.3 3.4 %all-to-all-start.1 = ((bf16[128,4,256]{0,2,1:T(8,128)(2,1)}), bf16[128,4,256]{0,2,1:T(8,128)(2,1)S(1)}, u32[]{:S(2)}, u32[]{:S(2)}) async-start(bf16[128,4,256]{0,2,1:T(8,128)(2,1)} %bitcast.3), calls=%async_computation.1 | async-start | bytes 524288 | tf_op jit(solution)/shard_map/all_to_all | solution.py:46
  27.7 1.8 %copy.19 = bf16[1,128,1024]{1,2,0:T(8,128)(2,1)} copy(bf16[1,128,1024]{2,1,0:T(8,128)(2,1)} %param.7) | data formatting | bytes 524288 | tf_op args[2]
  29.5 5.2 %all-to-all-done.1 = bf16[128,4,256]{0,2,1:T(8,128)(2,1)S(1)} async-done(((bf16[128,4,256]{0,2,1:T(8,128)(2,1)}), bf16[128,4,256]{0,2,1:T(8,128)(2,1)S(1)}, u32[]{:S(2)}, u32[]{:S(2)}) %all-to-all-start.1) | async-done | bytes 262176 | tf_op jit(solution)/shard_map/all_to_all | solution.py:46
  34.7 3.4 %all-to-all-start.2 = ((bf16[128,4,256]{0,2,1:T(8,128)(2,1)}), bf16[128,4,256]{0,2,1:T(8,128)(2,1)S(1)}, u32[]{:S(2)}, u32[]{:S(2)}) async-start(bf16[128,4,256]{0,2,1:T(8,128)(2,1)} %bitcast.7), calls=%async_computation.2 | async-start | bytes 524288 | tf_op jit(solution)/shard_map/all_to_all | solution.py:47
  38.1 0.1 iota_compare_fusion
  38.2 0.2 copy.16
  38.4 0.1 reshape.37
  38.5 0.2 copy.18
  38.8 0.1 reshape.38
  38.9 6.0 %all-to-all-done.2 = bf16[128,4,256]{0,2,1:T(8,128)(2,1)S(1)} async-done(((bf16[128,4,256]{0,2,1:T(8,128)(2,1)}), bf16[128,4,256]{0,2,1:T(8,128)(2,1)S(1)}, u32[]{:S(2)}, u32[]{:S(2)}) %all-to-all-start.2) | async-done | bytes 262176 | tf_op jit(solution)/shard_map/all_to_all | solution.py:47
  44.9 0.2 copy.20
  45.1 0.1 reshape.39
  45.2 0.0 copy-done
  45.2 2.2 %fusion.37 = f32[4,512]{1,0:T(4,128)S(1)} fusion(f32[4,512]{1,0:T(4,128)S(1)} %bitcast.61, pred[512,512]{0,1:T(8,128)(4,1)S(1)} %iota_compare_fusion, bf16[512,4,64]{0,2,1:T(8,128)(2,1)S(1)} %reshape.38, bf16[512,4,64]{0,2,1:T(8,128)(2,1)S(1)} %reshape.37), kind=kOutput, calls=%fused_computation.27 | convolution fusion | flops 140509696 | bytes 802816 | tf_op jit(solution)/shard_map/while/body/eval_jaxpr/sub | solution.py:33
  47.4 2.2 %fusion.10 = bf16[1,512,4,64]{1,3,2,0:T(8,128)(2,1)S(1)} fusion(f32[4,512]{1,0:T(4,128)S(1)} %fusion.37, bf16[512,4,64]{0,2,1:T(8,128)(2,1)S(1)} %reshape.39, f32[4,512]{1,0:T(4,128)S(1)} %bitcast.62, pred[512,512]{0,1:T(8,128)(4,1)S(1)} %iota_compare_fusion, bf16[512,4,64]{0,2,1:T(8,128)(2,1)S(1)} %reshape.38, bf16[512,4,64]{0,2,1:T(8,128)(2,1)S(1)} %reshape.37), kind=kOutput, calls=%fused_computation.14 | convolution fusion | flops 275909120 | bytes 1327104 | tf_op jit(solution)/shard_map/while/body/eval_jaxpr/hqk,hkd->hqd/dot_general | solution.py:35
  49.6 0.1 all_to_all.59
  49.7 10.4 %all_to_all.67 = bf16[4,128,256]{1,2,0:T(8,128)(2,1)S(1)} all-to-all(bf16[4,128,256]{1,2,0:T(8,128)(2,1)S(1)} %copy.22), channel_id=1, replica_groups=mesh['sp'=4,'dp'=8] {'sp'}, dimensions={0} | all-to-all | bytes 524288 | tf_op jit(solution)/shard_map/all_to_all | solution.py:50
  60.1 0.0 all-gather.2.cloned.1.call-done
  60.1 3.7 %fusion.2 = bf16[1,128,2048]{2,1,0:T(8,128)(2,1)} fusion(bf16[128,1024]{0,1:T(8,128)(2,1)S(1)} %bitcast.57, bf16[1024,2048]{1,0:T(8,128)(2,1)} %all-gather.2.cloned.1.call-done), kind=kOutput, calls=%fused_computation.6 | convolution fusion | flops 537133056 | bytes 4980736 | tf_op jit(solution)/shard_map/dot_general | solution.py:51
  (1 shorter events, 0.0 us)
Async XLA Ops:
  6.5 38.7 %copy-start = (f32[1,4,512]{2,1,0:T(4,128)S(1)}, f32[1,4,512]{2,1,0:T(4,128)}, u32[]{:S(2)}) copy-start(f32[1,4,512]{2,1,0:T(4,128)} %param.8) | copy-start | bytes 24580
  6.5 53.5 %all-gather.2.cloned.1.call-start = ((), (), s32[]{:S(2)}) async-start(), calls=%async_computation.4 | async-start | bytes 4718592 | tf_op jit(solution)/shard_map/all_gather | solution.py:53
  9.0 15.3 %all-to-all-start = ((bf16[128,4,256]{0,2,1:T(8,128)(2,1)}), bf16[128,4,256]{0,2,1:T(8,128)(2,1)S(1)}, u32[]{:S(2)}, u32[]{:S(2)}) async-start(bf16[128,4,256]{0,2,1:T(8,128)(2,1)} %bitcast), calls=%async_computation | async-start | bytes 524288 | tf_op jit(solution)/shard_map/all_to_all | solution.py:45
  24.3 10.4 %all-to-all-start.1 = ((bf16[128,4,256]{0,2,1:T(8,128)(2,1)}), bf16[128,4,256]{0,2,1:T(8,128)(2,1)S(1)}, u32[]{:S(2)}, u32[]{:S(2)}) async-start(bf16[128,4,256]{0,2,1:T(8,128)(2,1)} %bitcast.3), calls=%async_computation.1 | async-start | bytes 524288 | tf_op jit(solution)/shard_map/all_to_all | solution.py:46
  34.7 10.2 %all-to-all-start.2 = ((bf16[128,4,256]{0,2,1:T(8,128)(2,1)}), bf16[128,4,256]{0,2,1:T(8,128)(2,1)S(1)}, u32[]{:S(2)}, u32[]{:S(2)}) async-start(bf16[128,4,256]{0,2,1:T(8,128)(2,1)} %bitcast.7), calls=%async_computation.2 | async-start | bytes 524288 | tf_op jit(solution)/shard_map/all_to_all | solution.py:47
Sparse Core Ops, SparseCore 0:
  9.2 40.0 all-gather.1
where the time goes:
time: 71.1 us; the launch traced here: 70.6 us
  waiting for transfers between devices  19.1 us (27%)
  between operations  13.5 us (19%)
  starting transfers between devices  13.2 us (19%)
  blocking collectives  10.4 us (15%)
  matrix products  8.1 us (11%)
  local copies, waits for them, and re-layouts  6.39 us (9%)
    all_to_all x1, blocking collectives, shards(): lax.all_to_all(head_out, 'sp', split_axis=0, concat_axis=1, tiled=True)  10.4 us
    all_to_all x1, waiting for transfers between devices, shards(): lax.all_to_all(queries[0], 'sp', split_axis=1, concat_axis=0, tiled=True)  7.12 us
    all_to_all x1, starting transfers between devices, shards(): lax.all_to_all(queries[0], 'sp', split_axis=1, concat_axis=0, tiled=True)  6.35 us
    all_to_all x1, waiting for transfers between devices, shards(): lax.all_to_all(values[0], 'sp', split_axis=1, concat_axis=0, tiled=True)  6.01 us
    unnamed x5, local copies, waits for them, and re-layouts  5.36 us
    all_to_all x1, waiting for transfers between devices, shards(): lax.all_to_all(keys[0], 'sp', split_axis=1, concat_axis=0, tiled=True)  5.21 us
    dot_general x1, matrix products, shards(): jnp.dot(token_rows, lax.all_gather(out_weight, 'dp', axis=1, tiled=True),...  3.72 us
    all_to_all x1, starting transfers between devices, shards(): lax.all_to_all(keys[0], 'sp', split_axis=1, concat_axis=0, tiled=True)  3.41 us
  transfers between devices with their start and end apart: 4, of which 3 were waited for; matrix products, arithmetic and copies ran while one was open for 15% of the time, Pallas kernels for 0%

commit v1 on v0

--- a/solution.py
+++ b/solution.py
@@ -1,6 +1,10 @@
+import functools
+
 import jax
 import jax.numpy as jnp
 from jax import lax
+from jax.experimental import pallas as pl
+from jax.experimental.pallas import tpu as pltpu
 from jax.sharding import PartitionSpec as P
 
 
@@ -56,6 +60,416 @@
     return mixed_rows.astype(jnp.bfloat16)[None]
 
 
+MESH = pl.DeviceIdType.MESH
+LANES = 128
+HUB = 1
+
+
+def flip(index, bit):
+    return index + bit - 2 * bit * (lax.div(index, bit) % 2)
+
+
+def head_pair(q, ks, vs, gates, first_key, row_block, scale, head_size, causal):
+    rows = q.shape[0]
+    even = lax.broadcasted_iota(jnp.int32, (rows, LANES), 1) < head_size
+    q = q * jnp.asarray(scale, q.dtype)
+    zero = jnp.zeros_like(q)
+    stacked = jnp.concatenate([jnp.where(even, q, zero), jnp.where(even, zero, q)], axis=0)
+    k = ks[0] if len(ks) == 1 else jnp.concatenate(ks, axis=0)
+    v = vs[0] if len(vs) == 1 else jnp.concatenate(vs, axis=0)
+    span = k.shape[0]
+    scores = lax.dot_general(
+        stacked, k, (((1,), (1,)), ((), ())), preferred_element_type=jnp.float32
+    )
+    key_gates = gates[:, pl.ds(pl.multiple_of(first_key * rows, LANES), span)]
+    row_gates = gates[:, pl.ds(pl.multiple_of(row_block * rows, LANES), rows)].T
+    parts = []
+    for n in range(2):
+        part = scores[n * rows : (n + 1) * rows] + (
+            row_gates[:, 8 * n : 8 * n + 1] - key_gates[8 * n : 8 * n + 1]
+        )
+        if causal:
+            row = lax.broadcasted_iota(jnp.int32, (rows, span), 0) + (span - rows)
+            col = lax.broadcasted_iota(jnp.int32, (rows, span), 1)
+            part = jnp.where(col <= row, part, -jnp.inf)
+        parts.append(part)
+    tops = [jnp.max(part, axis=1, keepdims=True) for part in parts]
+    probs = jnp.concatenate(
+        [jnp.exp(part - top).astype(v.dtype) for part, top in zip(parts, tops)], axis=0
+    )
+    wide = jnp.concatenate([v, jnp.ones((span, LANES), v.dtype)], axis=1)
+    sums = jnp.dot(probs, wide, preferred_element_type=jnp.float32)
+    total = jnp.where(even, sums[:rows, LANES:], sums[rows:, LANES:])
+    result = jnp.where(even, sums[:rows, :LANES], sums[rows:, :LANES]) / total
+    top = jnp.where(even, tops[0], tops[1])
+    return result, top + jnp.log(total)
+
+
+def layer_kernel(
+    sizes, q_hbm, k_hbm, v_hbm, g_hbm, w_hbm, out_ref,
+    q_own, q_in, k_buf, v_buf, g_in, g_pair, o_out, s_out, o_in, s_in, o_own, s_own, heads, w_buf,
+    q_ss, q_rs, kv_ss, kv_rs, o_ss, o_rs, s_ss, s_rs, g_ss, g_rs, w_ss, w_rs, loc,
+):
+    sp, chunks, head_size, scale = sizes
+    z, d = lax.axis_index("sp"), lax.axis_index("dp")
+    rows = q_own.shape[0]
+    half = w_buf.shape[1] // 2
+    core, xs, ys = flip(d, 1), flip(d, 2), flip(d, 4)
+
+    def cols(c):
+        return pl.ds(pl.multiple_of(c * LANES, LANES), LANES)
+
+    def remote(src, dst, ss, rs, **device):
+        return pltpu.make_async_remote_copy(
+            src_ref=src, dst_ref=dst, send_sem=ss, recv_sem=rs,
+            device_id=device, device_id_type=MESH,
+        )
+
+    local = [
+        pltpu.make_async_copy(q_hbm.at[0], q_own, loc.at[0]),
+        pltpu.make_async_copy(k_hbm.at[0], k_buf.at[1], loc.at[1]),
+        pltpu.make_async_copy(v_hbm.at[0], v_buf.at[1], loc.at[2]),
+        pltpu.make_async_copy(g_hbm.at[0], g_in.at[z], loc.at[3]),
+        pltpu.make_async_copy(w_hbm, w_buf.at[0], loc.at[4]),
+    ]
+    for copy in local:
+        copy.start()
+
+    barrier = pltpu.get_barrier_semaphore()
+    for step in range(1, sp):
+        pl.semaphore_signal(
+            barrier, inc=1, device_id={"sp": lax.rem(z + step, sp)}, device_id_type=MESH
+        )
+    for peer in (core, xs, ys):
+        pl.semaphore_signal(barrier, inc=1, device_id={"dp": peer}, device_id_type=MESH)
+    pl.semaphore_wait(barrier, sp - 1 + 3)
+
+    def gate_copy(step):
+        return remote(
+            g_hbm.at[0], g_in.at[z], g_ss.at[step], g_rs.at[z], sp=lax.rem(z + step, sp)
+        )
+
+    for step in range(1, sp):
+        gate_copy(step).start()
+
+    def q_copy(c, slot, way, target):
+        return remote(
+            q_hbm.at[0, :, cols(c)], q_in.at[slot, :, cols(c)],
+            q_ss.at[way, c], q_rs.at[slot, c], sp=target,
+        )
+
+    def k_copy(c):
+        return remote(
+            k_hbm.at[0, :, cols(c)], k_buf.at[0, :, cols(c)],
+            kv_ss.at[0, c], kv_rs.at[0, c], sp=HUB,
+        )
+
+    def v_copy(c):
+        return remote(
+            v_hbm.at[0, :, cols(c)], v_buf.at[0, :, cols(c)],
+            kv_ss.at[1, c], kv_rs.at[1, c], sp=HUB,
+        )
+
+    @pl.when(z == 0)
+    def _():
+        for c in range(chunks):
+            k_copy(c).start()
+            v_copy(c).start()
+
+    @pl.when(z == HUB + 1)
+    def _():
+        for c in range(chunks):
+            q_copy(c, 0, 0, HUB).start()
+
+    @pl.when(z == HUB + 2)
+    def _():
+        for c in range(chunks):
+            q_copy(c, 1, 0, HUB).start()
+            q_copy(c, 1, 1, HUB + 1).start()
+
+    def w_copy(number, slot, part, bit, peer):
+        span = pl.ds(part * half, half)
+        src = w_hbm.at[span] if slot == 0 else w_buf.at[slot, span]
+        return remote(
+            src, w_buf.at[slot ^ bit, span], w_ss.at[number], w_rs.at[slot ^ bit, part], dp=peer
+        )
+
+    w_plan = {
+        "first": [(0, 0, 0, 2, xs), (1, 0, 1, 4, ys), (2, 0, 1, 2, xs), (3, 0, 0, 4, ys),
+                  (4, 0, 0, 1, core), (5, 0, 1, 1, core)],
+        "early": [(6, 2, 0, 4, ys), (7, 4, 1, 2, xs), (8, 2, 0, 1, core), (9, 4, 1, 1, core)],
+        "middle": [(10, 2, 1, 1, core), (11, 4, 0, 1, core)],
+        "late": [(12, 6, 0, 1, core), (13, 6, 1, 1, core)],
+    }
+
+    def w_arrived(slot, part):
+        span = pl.ds(part * half, half)
+        remote(
+            w_hbm.at[span], w_buf.at[slot, span], w_ss.at[0], w_rs.at[slot, part], dp=core
+        ).wait_recv()
+
+    def relay(stage):
+        seen = []
+        for number, slot, part, bit, peer in w_plan[stage]:
+            if slot and (slot, part) not in seen:
+                w_arrived(slot, part)
+                seen.append((slot, part))
+            w_copy(number, slot, part, bit, peer).start()
+
+    relay("first")
+
+    local[3].wait()
+    for owner in range(sp):
+        @pl.when(z != owner)
+        def _():
+            remote(
+                g_hbm.at[0], g_in.at[owner], g_ss.at[0], g_rs.at[owner], sp=lax.rem(z + 1, sp)
+            ).wait_recv()
+    per = g_in.shape[1]
+    for c in range(chunks):
+        for n in range(2):
+            head = 2 * c + n
+            line = g_in[head // per, head % per : head % per + 1, :]
+            g_pair[c, 8 * n : 8 * n + 8, :] = jnp.broadcast_to(line, (8, line.shape[1]))
+    for copy in local[:3]:
+        copy.wait()
+
+    def attend(c, q, slots, first_key, row_block, causal):
+        return head_pair(
+            q[:, cols(c)], [k_buf[s, :, cols(c)] for s in slots],
+            [v_buf[s, :, cols(c)] for s in slots],
+            g_pair.at[c], first_key, row_block, scale, head_size, causal,
+        )
+
+    def put(c, slot, result, lse):
+        o_out[slot, :, cols(c)] = result.astype(o_out.dtype)
+        turned = lse.T
+        s_out[slot, c, 0:8, :] = turned[0:8]
+        s_out[slot, c, 8:16, :] = turned[head_size : head_size + 8]
+
+    def o_copy(c, slot, into, target):
+        return remote(
+            o_out.at[slot, :, cols(c)], o_in.at[into, :, cols(c)],
+            o_ss.at[slot, c], o_rs.at[into, c], sp=target,
+        )
+
+    def s_copy(c, slot, into, target):
+        return remote(
+            s_out.at[slot, c], s_in.at[into, c], s_ss.at[slot, c], s_rs.at[into, c], sp=target
+        )
+
+    def give(c, slot, into, target):
+        s_copy(c, slot, into, target).start()
+        o_copy(c, slot, into, target).start()
+
+    def early(c):
+        @pl.when(c == chunks // 2)
+        def _():
+            relay("early")
+
+    @pl.when(z == 0)
+    def _():
+        @pl.loop(0, chunks)
+        def _(c):
+            early(c)
+            result, _lse = attend(c, q_own, [1], z, z, True)
+            heads[:, cols(c)] = result.astype(heads.dtype)
+
+    @pl.when(z == HUB)
+    def _():
+        @pl.loop(0, chunks)
+        def _(c):
+            early(c)
+            k_copy(c).wait_recv()
+            v_copy(c).wait_recv()
+            q_copy(c, 1, 0, HUB).wait_recv()
+            put(c, 1, *attend(c, q_in.at[1], [0, 1], 0, HUB + 2, False))
+            q_copy(c, 0, 0, HUB).wait_recv()
+            put(c, 0, *attend(c, q_in.at[0], [0, 1], 0, HUB + 1, False))
+            give(c, 1, 0, HUB + 2)
+            result, _lse = attend(c, q_own, [0, 1], 0, z, True)
+            heads[:, cols(c)] = result.astype(heads.dtype)
+            give(c, 0, 0, HUB + 1)
+
+    @pl.when(z > HUB)
+    def _():
+        @pl.loop(0, chunks)
+        def _(c):
+            early(c)
+
+            @pl.when(z == HUB + 1)
+            def _():
+                q_copy(c, 1, 1, HUB + 1).wait_recv()
+                put(c, 1, *attend(c, q_in.at[1], [1], z, HUB + 2, False))
+
+            result, lse = attend(c, q_own, [1], z, z, True)
+            o_own[:, cols(c)] = result
+            s_own[:, cols(c)] = lse
+
+            @pl.when(z == HUB + 1)
+            def _():
+                give(c, 1, 1, HUB + 2)
+
+    def taken(c, into):
+        s_copy(c, 0, into, HUB).wait_recv()
+        o_copy(c, 0, into, HUB).wait_recv()
+        turned = s_in[into, c].T
+        even = lax.broadcasted_iota(jnp.int32, (rows, LANES), 1) < head_size
+        lse = jnp.where(even, turned[:, 0:1], turned[:, 8:9])
+        return o_in[into, :, cols(c)].astype(jnp.float32), lse
+
+    def merge(first, second):
+        (a, la), (b, lb) = first, second
+        top = jnp.maximum(la, lb)
+        wa, wb = jnp.exp(la - top), jnp.exp(lb - top)
+        total = wa + wb
+        return (a * wa + b * wb) / total, top + jnp.log(total)
+
+    @pl.when(z <= HUB)
+    def _():
+        relay("middle")
+
+    @pl.when(z > HUB)
+    def _():
+        @pl.loop(0, chunks)
+        def _(c):
+            @pl.when(c == chunks // 2 + 1)
+            def _():
+                relay("middle")
+
+            @pl.when(z == HUB + 2)
+            def _():
+                result, lse = merge((o_own[:, cols(c)], s_own[:, cols(c)]), taken(c, 1))
+                o_own[:, cols(c)] = result
+                s_own[:, cols(c)] = lse
+
+            result, _lse = merge((o_own[:, cols(c)], s_own[:, cols(c)]), taken(c, 0))
+            heads[:, cols(c)] = result.astype(heads.dtype)
+
+        relay("late")
+
+    width = w_buf.shape[2]
+
+    def project(slot):
+        owner = d
+        for bit in (1, 2, 4):
+            if slot & bit:
+                owner = flip(owner, bit)
+        block = jnp.dot(heads[...], w_buf[slot], preferred_element_type=jnp.float32)
+        out_ref[0, :, pl.ds(pl.multiple_of(owner * width, LANES), width)] = block.astype(
+            out_ref.dtype
+        )
+
+    local[4].wait()
+    project(0)
+    for part in range(2):
+        w_arrived(1, part)
+    project(1)
+    project(2)
+    project(4)
+    for slot in (3, 5):
+        for part in range(2):
+            w_arrived(slot, part)
+        project(slot)
+
+    @pl.when(z <= HUB)
+    def _():
+        relay("late")
+
+    project(6)
+    for part in range(2):
+        w_arrived(7, part)
+    project(7)
+
+    for step in range(1, sp):
+        gate_copy(step).wait_send()
+    for stage in w_plan.values():
+        for entry in stage:
+            w_copy(*entry).wait_send()
+
+    @pl.when(z == 0)
+    def _():
+        for c in range(chunks):
+            k_copy(c).wait_send()
+            v_copy(c).wait_send()
+
+    @pl.when(z > HUB)
+    def _():
+        for c in range(chunks):
+            q_copy(c, 0, 0, HUB).wait_send()
+
+    @pl.when(z == HUB + 2)
+    def _():
+        for c in range(chunks):
+            q_copy(c, 1, 1, HUB + 1).wait_send()
+
+    @pl.when((z == HUB) | (z == HUB + 1))
+    def _():
+        for c in range(chunks):
+            s_copy(c, 1, 0, HUB + 2).wait_send()
+            o_copy(c, 1, 0, HUB + 2).wait_send()
+
+    @pl.when(z == HUB)
+    def _():
+        for c in range(chunks):
+            s_copy(c, 0, 0, HUB + 1).wait_send()
+            o_copy(c, 0, 0, HUB + 1).wait_send()
+
+
+def fused_shards(sp, queries, keys, values, cum_gates, out_weight):
+    _, rows, width = queries.shape
+    _, per, length = cum_gates.shape
+    head_size = width // (per * sp)
+    depth, block = out_weight.shape
+    dp = 8
+    chunks = width // LANES
+    bf16, f32 = queries.dtype, jnp.float32
+    dma = pltpu.SemaphoreType.DMA
+    return pl.pallas_call(
+        functools.partial(layer_kernel, (sp, chunks, head_size, head_size ** (-0.5))),
+        out_shape=jax.ShapeDtypeStruct((1, rows, block * dp), bf16),
+        in_specs=[pl.BlockSpec(memory_space=pl.ANY)] * 5,
+        out_specs=pl.BlockSpec(memory_space=pltpu.VMEM),
+        scratch_shapes=[
+            pltpu.VMEM((rows, width), bf16),
+            pltpu.VMEM((2, rows, width), bf16),
+            pltpu.VMEM((2, rows, width), bf16),
+            pltpu.VMEM((2, rows, width), bf16),
+            pltpu.VMEM((sp, per, length), f32),
+            pltpu.VMEM((chunks, 16, length), f32),
+            pltpu.VMEM((2, rows, width), bf16),
+            pltpu.VMEM((2, chunks, 16, LANES), f32),
+            pltpu.VMEM((2, rows, width), bf16),
+            pltpu.VMEM((2, chunks, 16, LANES), f32),
+            pltpu.VMEM((rows, width), f32),
+            pltpu.VMEM((rows, width), f32),
+            pltpu.VMEM((rows, width), bf16),
+            pltpu.VMEM((dp, depth, block), bf16),
+            dma((2, chunks)), dma((2, chunks)), dma((2, chunks)), dma((2, chunks)),
+            dma((2, chunks)), dma((2, chunks)), dma((2, chunks)), dma((2, chunks)),
+            dma((sp,)), dma((sp,)), dma((14,)), dma((dp, 2)), dma((5,)),
+        ],
+        compiler_params=pltpu.CompilerParams(collective_id=0, has_side_effects=True),
+        name="layer",
+    )(queries, keys, values, cum_gates, out_weight)
+
+
+def route(sp, dp, queries, keys, values, cum_gates, out_weight):
+    _, rows, width = queries.shape
+    head_size = width // (cum_gates.shape[1] * sp)
+    fits = (
+        sp == HUB + 3
+        and dp == 8
+        and rows == LANES
+        and 2 * head_size == LANES
+        and width % LANES == 0
+        and out_weight.shape[1] % LANES == 0
+    )
+    if fits:
+        return fused_shards(sp, queries, keys, values, cum_gates, out_weight)
+    return shards(queries, keys, values, cum_gates, out_weight)
+
+
 def solution(mesh):
     in_specs = (
         P("dp", "sp", None),
@@ -65,4 +479,5 @@
         P(None, "dp"),
     )
     out_specs = P("dp", "sp", None)
-    return jax.shard_map(shards, mesh=mesh, in_specs=in_specs, out_specs=out_specs, check_vma=False)
+    body = functools.partial(route, mesh.shape["sp"], mesh.shape["dp"])
+    return jax.shard_map(body, mesh=mesh, in_specs=in_specs, out_specs=out_specs, check_vma=False)

time: 71.1 us -> 30.4 us (0.43)
  the two profiles are of different devices: /device:TPU:0 before, /device:TPU:19 now
where the time goes in v1:
time: 30.4 us; the launch traced here: 30.3 us
  Pallas kernels  28.4 us (93%)
  local copies, waits for them, and re-layouts  1.88 us (6%)
    pallas_call x1, Pallas kernels, fused_shards(): pl.pallas_call(functools.partial(layer_kernel, (sp, chunks, head_size, he...  28.4 us
    unnamed x1, local copies, waits for them, and re-layouts  1.88 us

profile of v1, /device:TPU:19, one launch (start us, length us, event | category | flops | bytes accessed | tf_op | source)
XLA Modules:
  0.0 30.3 jit_solution(3768730119547459632)
XLA Ops:
  0.0 28.4 %layer.1 = bf16[1,128,2048]{2,1,0:T(8,128)(2,1)} custom-call(bf16[1,128,1024]{2,1,0:T(8,128)(2,1)} %q_hbm.1, bf16[1,128,1024]{2,1,0:T(8,128)(2,1)} %k_hbm.1, bf16[1,128,1024]{2,1,0:T(8,128)(2,1)} %v_hbm.1, f32[1,4,512]{2,1,0:T(4,128)} %g_hbm.1, bf16[1024,256]{1,0:T(8,128)(2,1)} %w_hbm.1), custom_call_target="tpu_custom_call" | custom-call | tf_op jit(solution)/shard_map/layer/pallas_call | solution.py:428
  28.4 1.9 %copy.7 = bf16[1,128,2048]{2,1,0:T(8,128)(2,1)} copy(bf16[1,128,2048]{2,1,0:T(8,128)(2,1)} %layer.1) | data formatting | bytes 1048576

commit v2 on v1

--- a/solution.py
+++ b/solution.py
@@ -108,7 +108,7 @@
 def layer_kernel(
     sizes, q_hbm, k_hbm, v_hbm, g_hbm, w_hbm, out_ref,
     q_own, q_in, k_buf, v_buf, g_in, g_pair, o_out, s_out, o_in, s_in, o_own, s_own, heads, w_buf,
-    q_ss, q_rs, kv_ss, kv_rs, o_ss, o_rs, s_ss, s_rs, g_ss, g_rs, w_ss, w_rs, loc,
+    q_ss, q_rs, kv_ss, kv_rs, o_ss, o_rs, s_ss, s_rs, g_ss, g_rs, w_ss, w_rs, loc, seen_sem,
 ):
     sp, chunks, head_size, scale = sizes
     z, d = lax.axis_index("sp"), lax.axis_index("dp")
@@ -136,62 +136,62 @@
         copy.start()
 
     barrier = pltpu.get_barrier_semaphore()
-    for step in range(1, sp):
-        pl.semaphore_signal(
-            barrier, inc=1, device_id={"sp": lax.rem(z + step, sp)}, device_id_type=MESH
-        )
+    @pl.when(z > 0)
+    def _():
+        pl.semaphore_signal(barrier, inc=1, device_id={"sp": z - 1}, device_id_type=MESH)
+
+    @pl.when(z < sp - 1)
+    def _():
+        pl.semaphore_signal(barrier, inc=1, device_id={"sp": z + 1}, device_id_type=MESH)
+
     for peer in (core, xs, ys):
         pl.semaphore_signal(barrier, inc=1, device_id={"dp": peer}, device_id_type=MESH)
-    pl.semaphore_wait(barrier, sp - 1 + 3)
-
-    def gate_copy(step):
-        return remote(
-            g_hbm.at[0], g_in.at[z], g_ss.at[step], g_rs.at[z], sp=lax.rem(z + step, sp)
-        )
-
-    for step in range(1, sp):
-        gate_copy(step).start()
+    pl.semaphore_wait(
+        barrier, 3 + (z > 0).astype(jnp.int32) + (z < sp - 1).astype(jnp.int32)
+    )
+
+    for teller, pair in ((HUB + 1, (HUB, HUB + 2)), (HUB, (HUB - 1, HUB + 1))):
+        @pl.when(z == teller)
+        def _():
+            for target in pair:
+                pl.semaphore_signal(
+                    seen_sem.at[teller - HUB], inc=1, device_id={"sp": target},
+                    device_id_type=MESH,
+                )
+
+    def gate_copy(owner, target, relayed=0):
+        return remote(
+            g_in.at[owner], g_in.at[owner], g_ss.at[relayed, target], g_rs.at[owner], sp=target
+        )
+
+    def gate_sends(run):
+        for owner, target in ((0, 1), (1, 0), (1, 2), (2, 1), (2, 3), (3, 2)):
+            @pl.when(z == owner)
+            def _():
+                run(gate_copy(owner, target))
 
     def q_copy(c, slot, way, target):
         return remote(
-            q_hbm.at[0, :, cols(c)], q_in.at[slot, :, cols(c)],
+            q_own.at[:, cols(c)], q_in.at[slot, :, cols(c)],
             q_ss.at[way, c], q_rs.at[slot, c], sp=target,
         )
 
     def k_copy(c):
         return remote(
-            k_hbm.at[0, :, cols(c)], k_buf.at[0, :, cols(c)],
+            k_buf.at[1, :, cols(c)], k_buf.at[0, :, cols(c)],
             kv_ss.at[0, c], kv_rs.at[0, c], sp=HUB,
         )
 
     def v_copy(c):
         return remote(
-            v_hbm.at[0, :, cols(c)], v_buf.at[0, :, cols(c)],
+            v_buf.at[1, :, cols(c)], v_buf.at[0, :, cols(c)],
             kv_ss.at[1, c], kv_rs.at[1, c], sp=HUB,
         )
-
-    @pl.when(z == 0)
-    def _():
-        for c in range(chunks):
-            k_copy(c).start()
-            v_copy(c).start()
-
-    @pl.when(z == HUB + 1)
-    def _():
-        for c in range(chunks):
-            q_copy(c, 0, 0, HUB).start()
-
-    @pl.when(z == HUB + 2)
-    def _():
-        for c in range(chunks):
-            q_copy(c, 1, 0, HUB).start()
-            q_copy(c, 1, 1, HUB + 1).start()
 
     def w_copy(number, slot, part, bit, peer):
         span = pl.ds(part * half, half)
-        src = w_hbm.at[span] if slot == 0 else w_buf.at[slot, span]
-        return remote(
-            src, w_buf.at[slot ^ bit, span], w_ss.at[number], w_rs.at[slot ^ bit, part], dp=peer
+        return remote(
+            w_buf.at[slot, span], w_buf.at[slot ^ bit, span], w_ss.at[number], w_rs.at[slot ^ bit, part], dp=peer
         )
 
     w_plan = {
@@ -216,24 +216,64 @@
                 seen.append((slot, part))
             w_copy(number, slot, part, bit, peer).start()
 
+    local[4].wait()
     relay("first")
+    for copy in local[:3]:
+        copy.wait()
 
     local[3].wait()
+    gate_sends(lambda copy: copy.start())
+
+    @pl.when(z == 0)
+    def _():
+        for c in range(chunks):
+            k_copy(c).start()
+            v_copy(c).start()
+            if c == 0:
+                pl.semaphore_wait(seen_sem.at[0], 1)
+                gate_copy(0, 2).start()
+
+    @pl.when(z == HUB + 1)
+    def _():
+        for c in range(chunks):
+            q_copy(c, 0, 0, HUB).start()
+            if c == 0:
+                pl.semaphore_wait(seen_sem.at[0], 1)
+                gate_copy(2, 0).start()
+
+    @pl.when(z == HUB + 2)
+    def _():
+        q_copy(0, 1, 1, HUB + 1).start()
+        pl.semaphore_wait(seen_sem.at[1], 1)
+        gate_copy(3, 1).start()
+        q_copy(0, 1, 0, HUB).start()
+        q_copy(1, 1, 0, HUB).start()
+        for c in range(1, chunks):
+            q_copy(c, 1, 1, HUB + 1).start()
+            if c + 1 < chunks:
+                q_copy(c + 1, 1, 0, HUB).start()
+
+    @pl.when(z == HUB)
+    def _():
+        pl.semaphore_wait(seen_sem.at[1], 1)
+        gate_copy(1, 3).start()
+
     for owner in range(sp):
         @pl.when(z != owner)
         def _():
-            remote(
-                g_hbm.at[0], g_in.at[owner], g_ss.at[0], g_rs.at[owner], sp=lax.rem(z + 1, sp)
-            ).wait_recv()
+            gate_copy(owner, (owner + 1) % sp).wait_recv()
+
+    @pl.when(z == HUB)
+    def _():
+        gate_copy(0, 3, 1).start()
+        gate_copy(3, 0, 1).start()
+
     per = g_in.shape[1]
     for c in range(chunks):
         for n in range(2):
             head = 2 * c + n
             line = g_in[head // per, head % per : head % per + 1, :]
             g_pair[c, 8 * n : 8 * n + 8, :] = jnp.broadcast_to(line, (8, line.shape[1]))
-    for copy in local[:3]:
-        copy.wait()
-
     def attend(c, q, slots, first_key, row_block, causal):
         return head_pair(
             q[:, cols(c)], [k_buf[s, :, cols(c)] for s in slots],
@@ -360,7 +400,6 @@
             out_ref.dtype
         )
 
-    local[4].wait()
     project(0)
     for part in range(2):
         w_arrived(1, part)
@@ -381,8 +420,12 @@
         w_arrived(7, part)
     project(7)
 
-    for step in range(1, sp):
-        gate_copy(step).wait_send()
+    gate_sends(lambda copy: copy.wait_send())
+    for owner, target, relayed in ((0, 2, 0), (2, 0, 0), (1, 3, 0), (3, 1, 0), (0, 3, 1), (3, 0, 1)):
+        @pl.when(z == (HUB if relayed else owner))
+        def _():
+            gate_copy(owner, target, relayed).wait_send()
+
     for stage in w_plan.values():
         for entry in stage:
             w_copy(*entry).wait_send()
@@ -428,7 +471,7 @@
     return pl.pallas_call(
         functools.partial(layer_kernel, (sp, chunks, head_size, head_size ** (-0.5))),
         out_shape=jax.ShapeDtypeStruct((1, rows, block * dp), bf16),
-        in_specs=[pl.BlockSpec(memory_space=pl.ANY)] * 5,
+        in_specs=[pl.BlockSpec(memory_space=pltpu.HBM)] * 5,
         out_specs=pl.BlockSpec(memory_space=pltpu.VMEM),
         scratch_shapes=[
             pltpu.VMEM((rows, width), bf16),
@@ -447,11 +490,12 @@
             pltpu.VMEM((dp, depth, block), bf16),
             dma((2, chunks)), dma((2, chunks)), dma((2, chunks)), dma((2, chunks)),
             dma((2, chunks)), dma((2, chunks)), dma((2, chunks)), dma((2, chunks)),
-            dma((sp,)), dma((sp,)), dma((14,)), dma((dp, 2)), dma((5,)),
+            dma((2, sp)), dma((sp,)), dma((14,)), dma((dp, 2)), dma((5,)),
+            pltpu.SemaphoreType.REGULAR((2,)),
         ],
-        compiler_params=pltpu.CompilerParams(collective_id=0, has_side_effects=True),
+        compiler_params=pltpu.CompilerParams(collective_id=0, has_side_effects=True, vmem_limit_bytes=16 * 2**20),
         name="layer",
-    )(queries, keys, values, cum_gates, out_weight)
+    )(*(pltpu.with_memory_space_constraint(x, pltpu.HBM) for x in (queries, keys, values, cum_gates, out_weight)))
 
 
 def route(sp, dp, queries, keys, values, cum_gates, out_weight):

time: 30.4 us -> 28.4 us (0.934)
  local copies, waits for them, and re-layouts: 1.88 us -> 0.8 us
  Pallas kernels: 28.4 us -> 27.4 us
    unnamed x1, local copies, waits for them, and re-layouts: 1.88 us -> 0.8 us
    pallas_call x1, Pallas kernels: 28.4 us -> 27.4 us  [fused_shards(): pl.pallas_call(functools.partial(layer_kernel, (sp, chunks, head_size, he...]
where the time goes in v2:
time: 28.4 us; the launch traced here: 28.2 us
  Pallas kernels  27.4 us (96%)
  local copies, waits for them, and re-layouts  0.8 us (3%)
    pallas_call x1, Pallas kernels, fused_shards(): pl.pallas_call(functools.partial(layer_kernel, (sp, chunks, head_size, he...  27.4 us
    unnamed x1, local copies, waits for them, and re-layouts  0.8 us

profile of v2, /device:TPU:19, one launch (start us, length us, event | category | flops | bytes accessed | tf_op | source)
XLA Modules:
  0.0 28.2 jit_solution(2581309600854539350)
XLA Ops:
  0.0 27.4 %layer.1 = bf16[1,128,2048]{2,1,0:T(8,128)(2,1)S(1)} custom-call(bf16[1,128,1024]{2,1,0:T(8,128)(2,1)} %q_hbm.1, bf16[1,128,1024]{2,1,0:T(8,128)(2,1)} %k_hbm.1, bf16[1,128,1024]{2,1,0:T(8,128)(2,1)} %v_hbm.1, f32[1,4,512]{2,1,0:T(4,128)} %g_hbm.1, bf16[1024,256]{1,0:T(8,128)(2,1)} %w_hbm.1), custom_call_target="tpu_custom_call" | custom-call | tf_op jit(solution)/shard_map/layer/pallas_call | solution.py:471
  27.4 0.8 %copy.7 = bf16[1,128,2048]{2,1,0:T(8,128)(2,1)} copy(bf16[1,128,2048]{2,1,0:T(8,128)(2,1)S(1)} %layer.1) | data formatting | bytes 1048576
